TPU v7x, 128 devices: a whole 4x4x4 slice. The times are simulated.
128 devices in a mesh: rep: 2 (over z_hi), fs: 32 (over z_lo, y, x), tp: 2 (over core).
Axes of the slice: x: 4, y: 4, z: 4 (z_hi: 2, z_lo: 2; z = z_hi * 2 + z_lo), core: 2. Of those that a mesh axis runs over, the one named last changes fastest.
Arguments:
- tokens: bfloat16 [40960, 2048], P(('rep', 'fs', 'tp')), may hold values from -6 to 6
- mix_gain: float32 [2048], replicated, may hold values from 0.1 to 1.9
- w_bgate: bfloat16 [2048, 2048], P('fs', 'tp'), may hold values from -0.125 to 0.125
- w_cgate: bfloat16 [2048, 2048], P('fs', 'tp'), may hold values from -0.125 to 0.125
- w_value: bfloat16 [2048, 2048], P('fs', 'tp'), may hold values from -0.125 to 0.125
- conv_taps: float32 [3, 2048], replicated, may hold values from -3 to 3
- w_mixout: bfloat16 [2048, 2048], P('tp', 'fs'), may hold values from -0.125 to 0.125
- mlp_gain: float32 [2048], replicated, may hold values from 0.1 to 1.9
- w_gate: bfloat16 [2048, 2816], P('fs', 'tp'), may hold values from -0.125 to 0.125
- w_up: bfloat16 [2048, 2816], P('fs', 'tp'), may hold values from -0.125 to 0.125
- w_down: bfloat16 [2816, 2048], P('tp', 'fs'), may hold values from -0.109375 to 0.109375
Outputs:
- block_out: bfloat16 [40960, 2048], P(('rep', 'fs', 'tp'))
All inputs are finite; a program needn't handle non-finite values.
Results may differ from a plain program's by a relative error of at most 0.0085.
Values may be sent and summed in bfloat16 or wider, within the bound.
A program may use at most 128 MiB of HBM per device.

v0:
```python
import jax
import jax.numpy as jnp
from jax import lax
from jax.sharding import Mesh
from jax.sharding import PartitionSpec as P

FS = ("fs_0", "fs_1", "fs_2")
REP_FS_TP = ("rep", "fs_0", "fs_1", "fs_2", "tp")


def sent_to_all(array, axis):
    peers = lax.axis_size(axis)
    return lax.all_to_all(
        jnp.broadcast_to(array[None], (peers, *array.shape)), axis, 0, 0, tiled=True
    )


def in_order(blocks, dim):
    dims = list(blocks.shape[1:])
    dims[dim] *= blocks.shape[0]
    return jnp.moveaxis(blocks, 0, dim).reshape(dims)


def collect(array, axis, dim):
    blocks = sent_to_all(array, axis)
    return in_order(blocks, dim)


def stacked_from(array, axes, turns):
    blocks = array
    for k in turns:
        blocks = lax.all_gather(blocks, axes[k])
    done = turns[::-1]
    back = [done.index(k) for k in range(len(axes))]
    blocks = blocks.transpose(*back, *range(len(axes), blocks.ndim))
    return blocks.reshape(-1, *array.shape)


def gather_axes(array, axes, turns, dim):
    return in_order(stacked_from(array, axes, turns), dim)


def split_up(array, dim, peers):
    dims = array.shape
    blocks = array.reshape(*dims[:dim], peers, dims[dim] // peers, *dims[dim + 1 :])
    return jnp.moveaxis(blocks, dim, 0)


def summed_on_arrival(array, axis, dim):
    blocks = split_up(array, dim, lax.axis_size(axis))
    arrived = lax.all_to_all(blocks, axis, split_axis=0, concat_axis=0, tiled=True)
    return arrived.astype(jnp.float32).sum(axis=0)


def rms_scale(matrix, gain):
    values = matrix.astype(jnp.float32)
    factor = lax.rsqrt(jnp.mean(values * values, axis=-1, keepdims=True) + 1e-06)
    return values * factor * gain


def causal_taps(mixed, filters):
    length = mixed.shape[-2]
    widths = [(0, 0)] * (mixed.ndim - 2) + [(2, 0), (0, 0)]
    padded = jnp.pad(mixed, widths)
    return (
        filters[0] * padded[..., 0:length, :]
        + filters[1] * padded[..., 1 : length + 1, :]
        + filters[2] * padded[..., 2 : length + 2, :]
    )


def gather_rows(normed):
    return collect(normed, "tp", 0)


def project_in(gathered, stacked):
    return jnp.einsum(
        "td,kdc->ktc",
        gathered,
        lax.all_gather(stacked, FS, axis=1, tiled=True),
        preferred_element_type=jnp.float32,
    )


def collect_out(weight):
    return gather_axes(weight, FS, (0, 1, 2), 1)


def sum_parts(local_cols, weight):
    return summed_on_arrival(
        jnp.dot(local_cols, weight, preferred_element_type=jnp.float32).astype(jnp.bfloat16),
        "tp",
        0,
    )


def on_device(
    tokens, mix_gain, w_bgate, w_cgate, w_value, conv_taps, w_mixout, mlp_gain, w_gate, w_up, w_down
):
    normed = rms_scale(tokens, mix_gain).astype(jnp.bfloat16)
    gathered = gather_rows(normed)
    projected = project_in(gathered, jnp.stack([w_bgate, w_cgate, w_value])).astype(jnp.bfloat16)
    channels = projected.shape[2]
    channel_taps = lax.dynamic_slice_in_dim(conv_taps, lax.axis_index("tp") * channels, channels, 1)
    mixed_in = projected[1].astype(jnp.float32) * projected[2].astype(jnp.float32)
    gated = (projected[0].astype(jnp.float32) * causal_taps(mixed_in, channel_taps)).astype(
        jnp.bfloat16
    )
    residual = tokens.astype(jnp.float32) + sum_parts(gated, collect_out(w_mixout))
    normed_two = rms_scale(residual, mlp_gain).astype(jnp.bfloat16)
    gathered_two = gather_rows(normed_two)
    gate_up = project_in(gathered_two, jnp.stack([w_gate, w_up]))
    hidden = (jax.nn.silu(gate_up[0]) * gate_up[1]).astype(jnp.bfloat16)
    result = residual + 0.5 * sum_parts(hidden, collect_out(w_down))
    return result.astype(jnp.bfloat16)


def solution(mesh):
    finer = Mesh(
        mesh.devices.reshape(mesh.shape["rep"], 2, 4, 4, mesh.shape["tp"]),
        ("rep", "fs_0", "fs_1", "fs_2", "tp"),
    )
    return jax.shard_map(
        on_device,
        mesh=finer,
        in_specs=(
            P(REP_FS_TP, None),
            P(),
            P(FS, "tp"),
            P(FS, "tp"),
            P(FS, "tp"),
            P(),
            P("tp", FS),
            P(),
            P(FS, "tp"),
            P(FS, "tp"),
            P("tp", FS),
        ),
        out_specs=P(REP_FS_TP, None),
        check_vma=False,
    )
```

profile of v0, /device:TPU:1, one launch (start us, length us, event | category | flops | bytes accessed | tf_op | source)
XLA Modules:
  0.0 567.4 jit_solution(2443627094710564930)
XLA Ops:
  6.5 6.7 %all-gather = bf16[2048,64]{0,1:T(8,128)(2,1)S(1)} all-gather(bf16[1024,64]{0,1:T(8,128)(2,1)} %param.17), channel_id=2, replica_groups=mesh['rep'=2,'fs_0'=2,'fs_1'=4,'fs_2'=4,'tp'=2] {'fs_0'}, dimensions={0}, use_global_device_ids=true | all-gather | bytes 393216 | tf_op jit(solution)/shard_map/all_gather | solution.py:32
  13.3 0.7 copy.27
  14.1 5.9 %all-gather.3 = bf16[2816,64]{0,1:T(8,128)(2,1)S(1)} all-gather(bf16[1408,64]{0,1:T(8,128)(2,1)} %param.21), channel_id=5, replica_groups=mesh['rep'=2,'fs_0'=2,'fs_1'=4,'fs_2'=4,'tp'=2] {'fs_0'}, dimensions={0}, use_global_device_ids=true | all-gather | bytes 540672 | tf_op jit(solution)/shard_map/all_gather | solution.py:32
  20.0 0.8 copy.26
  20.8 18.1 %all-gather.17.cloned.1.call-done = bf16[8,1024,64]{1,2,0:T(8,128)(2,1)} async-done(((bf16[2,1024,64]{1,2,0:T(8,128)(2,1)}), bf16[8,1024,64]{1,2,0:T(8,128)(2,1)}) %all-gather.17.cloned.1.call-update) | async-done | bytes 1048592 | tf_op jit(solution)/shard_map/all_gather | solution.py:32
  39.0 29.2 %all-gather.21.cloned.1.call-done = bf16[8,1408,64]{1,2,0:T(8,128)(2,1)} async-done(((bf16[2,1408,64]{1,2,0:T(8,128)(2,1)}), bf16[8,1408,64]{1,2,0:T(8,128)(2,1)}) %all-gather.21.cloned.1.call-update) | async-done | bytes 1441808 | tf_op jit(solution)/shard_map/all_gather | solution.py:32
  68.4 0.8 pad_maximum_fusion
  69.3 0.8 pad_maximum_fusion.1
  70.8 1.9 broadcast_in_dim.4
  72.7 4.7 all-to-all-start
  77.4 0.9 constant_dynamic-slice_fusion
  78.3 40.2 %all-gather.19.cloned.1.call-done = bf16[16,2,1024,64]{2,3,1,0:T(8,128)(2,1)} async-done(((bf16[4,2,1024,64]{2,3,1,0:T(8,128)(2,1)}), bf16[16,2,1024,64]{2,3,1,0:T(8,128)(2,1)}) %all-gather.19.cloned.1.call-update) | async-done | bytes 4194320 | tf_op jit(solution)/shard_map/all_gather | solution.py:32
  118.5 4.9 copy.19
  123.4 58.3 %all-gather.23.cloned.1.call-done = bf16[16,2,1408,64]{2,3,1,0:T(8,128)(2,1)} async-done(((bf16[4,2,1408,64]{2,3,1,0:T(8,128)(2,1)}), bf16[16,2,1408,64]{2,3,1,0:T(8,128)(2,1)}) %all-gather.23.cloned.1.call-update) | async-done | bytes 5767184 | tf_op jit(solution)/shard_map/all_gather | solution.py:32
  181.7 5.7 %copy.21 = bf16[2,4,4,1408,64]{3,4,2,1,0:T(8,128)(2,1)} copy(bf16[2,4,4,1408,64]{3,4,0,1,2:T(8,128)(2,1)} %bitcast.63) | data formatting | bytes 11534336 | tf_op jit(solution)/shard_map/transpose | solution.py:35
  187.4 153.6 %all-gather.13.cloned.1.call-done = bf16[3,2048,1024]{2,1,0:T(8,128)(2,1)} async-done(((bf16[3,64,1024]{2,1,0:T(8,128)(2,1)}), bf16[3,2048,1024]{2,1,0:T(8,128)(2,1)}) %all-gather.13.cloned.1.call-update) | async-done | bytes 12582928 | tf_op jit(solution)/shard_map/all_gather | solution.py:80
  341.0 11.2 %convert_bitcast_fusion = bf16[3,640,1024]{2,1,0:T(8,128)(2,1)S(1)} fusion(bf16[640,2048,1]{1,0,2:T(8,128)(2,1)S(1)} %bitcast.67, bf16[3,2048,1024]{2,1,0:T(8,128)(2,1)} %all-gather.13.cloned.1.call-done), kind=kOutput, calls=%fused_computation.3 | convolution fusion | flops 8055029760 | bytes 19136512 | tf_op jit(solution)/shard_map/td,kdc->ktc/dot_general | solution.py:77
  352.2 0.5 multiply_bitcast_fusion
  352.8 1.7 copy-done.3
  354.4 3.5 convolution_convert_fusion.1
  357.9 23.8 %all_to_all.20 = bf16[2,320,2048]{2,1,0:T(8,128)(2,1)S(1)} all-to-all(bf16[2,320,2048]{2,1,0:T(8,128)(2,1)S(1)} %bitcast.68), channel_id=1, replica_groups=mesh['rep'=2,'fs_0'=2,'fs_1'=4,'fs_2'=4,'tp'=2] {'tp'}, dimensions={0} | all-to-all | bytes 5242880 | tf_op jit(solution)/shard_map/all_to_all | solution.py:51
  381.7 0.6 convert_reduce_fusion.1
  382.3 0.7 copy-done.1
  384.2 1.9 broadcast_in_dim.5
  386.1 5.4 all-to-all-start.2
  391.5 120.2 %all-gather.15.cloned.1.call-done = bf16[2,2048,1408]{2,1,0:T(8,128)(2,1)} async-done(((bf16[2,64,1408]{2,1,0:T(8,128)(2,1)}), bf16[2,2048,1408]{2,1,0:T(8,128)(2,1)}) %all-gather.15.cloned.1.call-update) | async-done | bytes 11534352 | tf_op jit(solution)/shard_map/all_gather | solution.py:80
  511.6 13.1 %convolution_bitcast_fusion = f32[2,640,1408]{1,2,0:T(8,128)S(1)} fusion(bf16[2,2048,1408]{2,1,0:T(8,128)(2,1)} %all-gather.15.cloned.1.call-done, bf16[640,2048,1]{1,0,2:T(8,128)(2,1)} %bitcast.21), kind=kOutput, calls=%fused_computation.2 | convolution fusion | flops 7381975040 | bytes 21364736 | tf_op jit(solution)/shard_map/td,kdc->ktc/dot_general | solution.py:77
  524.7 7.0 %convolution_convert_fusion = bf16[640,2048]{1,0:T(8,128)(2,1)S(1)} fusion(bf16[1408,2048]{0,1:T(8,128)(2,1)} %bitcast.64, f32[2,640,1408]{1,2,0:T(8,128)S(1)} %convolution_bitcast_fusion), kind=kOutput, calls=%fused_computation.9 | convolution fusion | flops 3697704960 | bytes 15597568 | tf_op jit(solution)/shard_map/dot_general | solution.py:91
  531.7 25.7 %all_to_all.21 = bf16[2,320,2048]{2,1,0:T(8,128)(2,1)S(1)} all-to-all(bf16[2,320,2048]{2,1,0:T(8,128)(2,1)S(1)} %bitcast.69), channel_id=1, replica_groups=mesh['rep'=2,'fs_0'=2,'fs_1'=4,'fs_2'=4,'tp'=2] {'tp'}, dimensions={0} | all-to-all | bytes 5242880 | tf_op jit(solution)/shard_map/all_to_all | solution.py:51
  557.5 0.6 convert_reduce_fusion
  558.1 0.7 copy-done.2
  558.8 1.8 add_convert_fusion
  (39 shorter events, 2.2 us)
Async XLA Ops:
  6.5 61.8 %copy-start.8 = (bf16[64,1024]{1,0:T(8,128)(2,1)S(1)}, bf16[64,1024]{1,0:T(8,128)(2,1)}, u32[]{:S(2)}) copy-start(bf16[64,1024]{1,0:T(8,128)(2,1)} %param.13) | copy-start | bytes 393220
  6.5 61.8 %copy-start.7 = (bf16[64,1024]{1,0:T(8,128)(2,1)S(1)}, bf16[64,1024]{1,0:T(8,128)(2,1)}, u32[]{:S(2)}) copy-start(bf16[64,1024]{1,0:T(8,128)(2,1)} %param.14) | copy-start | bytes 393220
  6.5 61.8 %copy-start.6 = (bf16[64,1024]{1,0:T(8,128)(2,1)S(1)}, bf16[64,1024]{1,0:T(8,128)(2,1)}, u32[]{:S(2)}) copy-start(bf16[64,1024]{1,0:T(8,128)(2,1)} %param.15) | copy-start | bytes 393220
  6.5 32.4 %all-gather.17.cloned.1.call-start = ((), (), s32[]{:S(2)}) async-start(), calls=%async_computation.6 | async-start | bytes 1310720 | tf_op jit(solution)/shard_map/all_gather | solution.py:32
  14.0 55.2 %copy-start.4 = (bf16[64,1408]{1,0:T(8,128)(2,1)S(1)}, bf16[64,1408]{1,0:T(8,128)(2,1)}, u32[]{:S(2)}) copy-start(bf16[64,1408]{1,0:T(8,128)(2,1)} %param.20) | copy-start | bytes 540676
  14.0 55.2 %copy-start.5 = (bf16[64,1408]{1,0:T(8,128)(2,1)S(1)}, bf16[64,1408]{1,0:T(8,128)(2,1)}, u32[]{:S(2)}) copy-start(bf16[64,1408]{1,0:T(8,128)(2,1)} %param.19) | copy-start | bytes 540676
  14.0 54.2 %all-gather.21.cloned.1.call-start = ((), (), s32[]{:S(2)}) async-start(), calls=%async_computation.8 | async-start | bytes 1802240 | tf_op jit(solution)/shard_map/all_gather | solution.py:32
  20.7 49.4 %copy-start = (bf16[320,2048]{1,0:T(8,128)(2,1)S(1)}, bf16[320,2048]{1,0:T(8,128)(2,1)}, u32[]{:S(2)}) copy-start(bf16[320,2048]{1,0:T(8,128)(2,1)} %param.11) | copy-start | bytes 3932164
  20.7 97.8 %all-gather.19.cloned.1.call-start = ((), (), s32[]{:S(2)}) async-start(), calls=%async_computation.7 | async-start | bytes 5242880 | tf_op jit(solution)/shard_map/all_gather | solution.py:32
  39.0 31.5 %copy-start.9 = (f32[2048]{0:T(1024)S(1)}, f32[2048]{0:T(1024)}, u32[]{:S(2)}) copy-start(f32[2048]{0:T(1024)} %param.12) | copy-start | bytes 24580
  39.0 142.7 %all-gather.23.cloned.1.call-start = ((), (), s32[]{:S(2)}) async-start(), calls=%async_computation.9 | async-start | bytes 7208960 | tf_op jit(solution)/shard_map/all_gather | solution.py:32
  68.3 272.7 %all-gather.13.cloned.1.call-start = ((), (), s32[]{:S(2)}) async-start(), calls=%async_computation.4 | async-start | bytes 12976128 | tf_op jit(solution)/shard_map/all_gather | solution.py:80
  69.2 442.4 %all-gather.15.cloned.1.call-start = ((), (), s32[]{:S(2)}) async-start(), calls=%async_computation.5 | async-start | bytes 11894784 | tf_op jit(solution)/shard_map/all_gather | solution.py:80
  72.7 114.7 %all-to-all-start = ((bf16[2,320,2048]{2,1,0:T(8,128)(2,1)}), bf16[2,320,2048]{2,1,0:T(8,128)(2,1)S(1)}, u32[]{:S(2)}, u32[]{:S(2)}) async-start(bf16[2,320,2048]{2,1,0:T(8,128)(2,1)} %broadcast_in_dim.4), calls=%async_computation | async-start | bytes 5242880 | tf_op jit(solution)/shard_map/all_to_all | solution.py:13
  352.2 2.2 copy-start.3
  381.7 1.3 copy-start.1
  383.0 0.7 copy-start.10
  386.1 125.5 %all-to-all-start.2 = ((bf16[2,320,2048]{2,1,0:T(8,128)(2,1)}), bf16[2,320,2048]{2,1,0:T(8,128)(2,1)}, u32[]{:S(2)}, u32[]{:S(2)}) async-start(bf16[2,320,2048]{2,1,0:T(8,128)(2,1)} %broadcast_in_dim.5), calls=%async_computation.2 | async-start | bytes 5242880 | tf_op jit(solution)/shard_map/all_to_all | solution.py:13
  557.5 1.3 copy-start.2
Sparse Core Ops, SparseCore 0:
  14.1 24.7 all-gather.16
  40.6 27.6 all-gather.20
  69.9 48.5 all-gather.18
  120.0 61.5 all-gather.22
  183.1 157.7 all-gather.12
  342.5 169.0 all-gather.14
where the time goes:
time: 568 us; the launch traced here: 567 us
  waiting for transfers between devices  420 us (74%)
  blocking collectives  62.1 us (11%)
  matrix products  34.9 us (6%)
  local copies, waits for them, and re-layouts  20.1 us (4%)
  between operations  13.6 us (2%)
  starting transfers between devices  10.3 us (2%)
  other arithmetic  6.69 us (1%)
    all_gather x2, waiting for transfers between devices, project_in(): lax.all_gather(stacked, FS, axis=1, tiled=True)  274 us
    all_gather x4, waiting for transfers between devices, stacked_from(): blocks = lax.all_gather(blocks, axes[k])  146 us
    all_to_all x2, blocking collectives, summed_on_arrival(): lax.all_to_all(blocks, axis, split_axis=0, concat_axis=0, tiled=True)  49.5 us
    dot_general x2, matrix products, project_in(): jnp.einsum('td,kdc->ktc', gathered, lax.all_gather(stacked, FS, axis=1, t...  24.3 us
    all_gather x2, blocking collectives, stacked_from(): blocks = lax.all_gather(blocks, axes[k])  12.6 us
  transfers between devices with their start and end apart: 8, of which 6 were waited for; matrix products, arithmetic and copies ran while one was open for 6% of the time, Pallas kernels for 0%

commit v1 on v0

--- a/solution.py
+++ b/solution.py
@@ -74,11 +74,14 @@
 
 
 def project_in(gathered, stacked):
+
+    def edges_number(frame_in):
+        carry = jnp.stack([frame_in for _ in range(lax.axis_size(FS))], axis=0)
+        lower = lax.all_to_all(carry, axis_name=FS, split_axis=0, concat_axis=0)
+        return jnp.concatenate(lower, axis=1)
+
     return jnp.einsum(
-        "td,kdc->ktc",
-        gathered,
-        lax.all_gather(stacked, FS, axis=1, tiled=True),
-        preferred_element_type=jnp.float32,
+        "td,kdc->ktc", gathered, edges_number(stacked), preferred_element_type=jnp.float32
     )
 
 

time: 568 us -> 563 us (level)
  waiting for transfers between devices: 420 us -> 321 us
  starting transfers between devices: 10.3 us -> 46.4 us
  local copies, waits for them, and re-layouts: 20.1 us -> 49.6 us
  blocking collectives: 62.1 us -> 87.8 us
    all_gather x2 -> x0, waiting for transfers between devices: 274 us -> none  [project_in(): lax.all_gather(stacked, FS, axis=1, tiled=True)]
    all_gather x4, waiting for transfers between devices: 146 us -> 320 us  [stacked_from(): blocks = lax.all_gather(blocks, axes[k])]
    all_gather x2, blocking collectives: 12.6 us -> 69.9 us  [stacked_from(): blocks = lax.all_gather(blocks, axes[k])]
    all_to_all x0 -> x2, starting transfers between devices: none -> 40.5 us  [edges_number(): lower = lax.all_to_all(carry, axis_name=FS, split_axis=0, concat_axis=0)]
    all_to_all x2, blocking collectives: 49.5 us -> 11.5 us  [summed_on_arrival(): lax.all_to_all(blocks, axis, split_axis=0, concat_axis=0, tiled=True)]
    another operation x0 -> x2, local copies, waits for them, and re-layouts: none -> 12 us  [edges_number(): carry = jnp.stack([frame_in for _ in range(lax.axis_size(FS))], axis=0)]
    reshape x0 -> x1, local copies, waits for them, and re-layouts: none -> 10.7 us  [edges_number(): return jnp.concatenate(lower, axis=1)]
    all_to_all x0 -> x1, local copies, waits for them, and re-layouts: none -> 9.97 us  [edges_number(): lower = lax.all_to_all(carry, axis_name=FS, split_axis=0, concat_axis=0)]
  transfers between devices with their start and end apart: 8 -> 7, of which waited for: 6 -> 3; matrix products, arithmetic and copies ran while one was open for 6% -> 7% of each run, Pallas kernels for 0% -> 0%
where the time goes in v1:
time: 563 us; the launch traced here: 559 us
  waiting for transfers between devices  321 us (57%)
  blocking collectives  87.8 us (16%)
  local copies, waits for them, and re-layouts  49.6 us (9%)
  starting transfers between devices  46.4 us (8%)
  matrix products  34.9 us (6%)
  between operations  13.4 us (2%)
  other arithmetic  6.21 us (1%)
    all_gather x4, waiting for transfers between devices, stacked_from(): blocks = lax.all_gather(blocks, axes[k])  320 us
    all_gather x2, blocking collectives, stacked_from(): blocks = lax.all_gather(blocks, axes[k])  69.9 us
    all_to_all x2, starting transfers between devices, edges_number(): lower = lax.all_to_all(carry, axis_name=FS, split_axis=0, concat_axis=0)  40.5 us
    dot_general x2, matrix products, project_in(): jnp.einsum('td,kdc->ktc', gathered, edges_number(stacked), preferred_elem...  23.6 us
    another operation x2, local copies, waits for them, and re-layouts, edges_number(): carry = jnp.stack([frame_in for _ in range(lax.axis_size(FS))], axis=0)  12 us
    all_to_all x2, blocking collectives, summed_on_arrival(): lax.all_to_all(blocks, axis, split_axis=0, concat_axis=0, tiled=True)  11.5 us
    dot_general x2, matrix products, sum_parts(): jnp.dot(local_cols, weight, preferred_element_type=jnp.float32)  11.3 us
  transfers between devices with their start and end apart: 7, of which 3 were waited for; matrix products, arithmetic and copies ran while one was open for 7% of the time, Pallas kernels for 0%

profile of v1, /device:TPU:1, one launch (start us, length us, event | category | flops | bytes accessed | tf_op | source)
XLA Modules:
  0.0 559.3 jit_solution(10694746672683173550)
XLA Ops:
  6.5 1.0 pad_maximum_fusion.1
  7.6 5.8 %stack.26 = bf16[32,2,64,1408]{3,2,1,0:T(8,128)(2,1)} broadcast(bf16[2,64,1408]{2,1,0:T(8,128)(2,1)S(1)} %pad_maximum_fusion.1), dimensions={1,2,3} | broadcast | bytes 11894784 | tf_op jit(solution)/shard_map/stack | solution.py:79
  13.4 9.5 %all-to-all-start.3 = ((bf16[32,2,64,1408]{3,2,1,0:T(8,128)(2,1)}), bf16[32,2,64,1408]{3,2,1,0:T(8,128)(2,1)}, u32[]{:S(2)}, u32[]{:S(2)}) async-start(bf16[32,2,64,1408]{3,2,1,0:T(8,128)(2,1)} %stack.26), calls=%async_computation.3 | async-start | bytes 23068672 | tf_op jit(solution)/shard_map/all_to_all | solution.py:80
  23.0 64.3 %all-gather = bf16[2048,64]{0,1:T(8,128)(2,1)S(1)} all-gather(bf16[1024,64]{0,1:T(8,128)(2,1)S(1)} %copy-done.3), channel_id=2, replica_groups=mesh['rep'=2,'fs_0'=2,'fs_1'=4,'fs_2'=4,'tp'=2] {'fs_0'}, dimensions={0}, use_global_device_ids=true | all-gather | bytes 393216 | tf_op jit(solution)/shard_map/all_gather | solution.py:32
  87.3 0.7 copy.37
  88.1 5.6 all-gather.3
  93.7 0.8 copy.36
  94.6 98.7 %all-gather.11.cloned.1.call-done = bf16[8,1024,64]{1,2,0:T(8,128)(2,1)} async-done(((bf16[2,1024,64]{1,2,0:T(8,128)(2,1)}), bf16[8,1024,64]{1,2,0:T(8,128)(2,1)}) %all-gather.11.cloned.1.call-update) | async-done | bytes 1048592 | tf_op jit(solution)/shard_map/all_gather | solution.py:32
  193.3 6.1 %stack.22 = bf16[32,3,64,1024]{3,2,1,0:T(8,128)(2,1)} broadcast(bf16[3,64,1024]{2,1,0:T(8,128)(2,1)S(1)} %pad_maximum_fusion), dimensions={1,2,3} | broadcast | bytes 12976128 | tf_op jit(solution)/shard_map/stack | solution.py:79
  199.5 31.1 %all-to-all-start = ((bf16[32,3,64,1024]{3,2,1,0:T(8,128)(2,1)}), bf16[32,3,64,1024]{3,2,1,0:T(8,128)(2,1)}, u32[]{:S(2)}, u32[]{:S(2)}) async-start(bf16[32,3,64,1024]{3,2,1,0:T(8,128)(2,1)} %stack.22), calls=%async_computation | async-start | bytes 25165824 | tf_op jit(solution)/shard_map/all_to_all | solution.py:80
  230.7 0.5 all-gather.17.cloned.1.call-update
  231.2 0.9 constant_dynamic-slice_fusion
  232.8 118.6 %all-gather.13.cloned.1.call-done = bf16[16,2,1024,64]{2,3,1,0:T(8,128)(2,1)} async-done(((bf16[4,2,1024,64]{2,3,1,0:T(8,128)(2,1)}), bf16[16,2,1024,64]{2,3,1,0:T(8,128)(2,1)}) %all-gather.13.cloned.1.call-update) | async-done | bytes 4194320 | tf_op jit(solution)/shard_map/all_gather | solution.py:32
  351.4 4.9 copy.26
  356.3 103.2 %all-gather.17.cloned.1.call-done = bf16[16,2,1408,64]{2,3,1,0:T(8,128)(2,1)} async-done(((bf16[4,2,1408,64]{2,3,1,0:T(8,128)(2,1)}), bf16[16,2,1408,64]{2,3,1,0:T(8,128)(2,1)}) %all-gather.17.cloned.1.call-update) | async-done | bytes 5767184 | tf_op jit(solution)/shard_map/all_gather | solution.py:32
  459.5 5.7 %copy.30 = bf16[2,4,4,1408,64]{3,4,2,1,0:T(8,128)(2,1)} copy(bf16[2,4,4,1408,64]{3,4,0,1,2:T(8,128)(2,1)} %bitcast.75) | data formatting | bytes 11534336 | tf_op jit(solution)/shard_map/transpose | solution.py:35
  465.2 10.0 %copy.27 = bf16[32,2,64,1408]{3,2,0,1:T(8,128)(2,1)} copy(bf16[32,2,64,1408]{3,2,1,0:T(8,128)(2,1)} %all-to-all-done.3) | data formatting | bytes 23068672 | tf_op jit(solution)/shard_map/all_to_all | solution.py:80
  475.1 1.9 broadcast_in_dim.4
  477.1 5.7 %all-to-all-start.1 = ((bf16[2,320,2048]{2,1,0:T(8,128)(2,1)}), bf16[2,320,2048]{2,1,0:T(8,128)(2,1)}, u32[]{:S(2)}, u32[]{:S(2)}) async-start(bf16[2,320,2048]{2,1,0:T(8,128)(2,1)} %broadcast_in_dim.4), calls=%async_computation.1 | async-start | bytes 5242880 | tf_op jit(solution)/shard_map/all_to_all | solution.py:13
  482.8 10.7 %copy.24 = bf16[3,32,64,1024]{3,2,1,0:T(8,128)(2,1)} copy(bf16[3,32,64,1024]{3,2,0,1:T(8,128)(2,1)} %bitcast.3) | data formatting | bytes 25165824 | tf_op jit(solution)/shard_map/reshape | solution.py:81
  493.5 12.0 %convert_bitcast_fusion = bf16[3,640,1024]{2,1,0:T(8,128)(2,1)S(1)} fusion(bf16[640,2048,1]{1,0,2:T(8,128)(2,1)} %bitcast.6, bf16[3,2048,1024]{2,1,0:T(8,128)(2,1)} %bitcast.68), kind=kOutput, calls=%fused_computation.3 | convolution fusion | flops 8055029760 | bytes 19136512 | tf_op jit(solution)/shard_map/td,kdc->ktc/dot_general | solution.py:83
  505.6 0.5 multiply_bitcast_fusion
  506.1 1.7 copy-done.1
  507.7 3.5 convolution_convert_fusion.1
  511.2 5.7 %all_to_all.30 = bf16[2,320,2048]{2,1,0:T(8,128)(2,1)S(1)} all-to-all(bf16[2,320,2048]{2,1,0:T(8,128)(2,1)S(1)} %bitcast.78), channel_id=1, replica_groups=mesh['rep'=2,'fs_0'=2,'fs_1'=4,'fs_2'=4,'tp'=2] {'tp'}, dimensions={0} | all-to-all | bytes 5242880 | tf_op jit(solution)/shard_map/all_to_all | solution.py:51
  516.9 0.6 convert_reduce_fusion.1
  518.8 6.4 %all_to_all.31 = bf16[2,320,2048]{2,1,0:T(8,128)(2,1)S(1)} all-to-all(bf16[2,320,2048]{2,1,0:T(8,128)(2,1)S(1)} %broadcast_in_dim.5), channel_id=1, replica_groups=mesh['rep'=2,'fs_0'=2,'fs_1'=4,'fs_2'=4,'tp'=2] {'tp'}, dimensions={0} | all-to-all | bytes 5242880 | tf_op jit(solution)/shard_map/all_to_all | solution.py:13
  525.2 11.5 %convolution_bitcast_fusion = f32[2,640,1408]{1,2,0:T(8,128)} fusion(bf16[2,2048,1408]{2,1,0:T(8,128)(2,1)S(1)} %bitcast.71, bf16[640,2048,1]{1,0,2:T(8,128)(2,1)S(1)} %bitcast.79), kind=kOutput, calls=%fused_computation.2 | convolution fusion | flops 7381975040 | bytes 21364736 | tf_op jit(solution)/shard_map/td,kdc->ktc/dot_general | solution.py:83
  536.8 7.8 %convolution_convert_fusion = bf16[640,2048]{1,0:T(8,128)(2,1)S(1)} fusion(bf16[1408,2048]{0,1:T(8,128)(2,1)S(1)} %bitcast.74, f32[2,640,1408]{1,2,0:T(8,128)} %convolution_bitcast_fusion), kind=kOutput, calls=%fused_computation.9 | convolution fusion | flops 3697704960 | bytes 15597568 | tf_op jit(solution)/shard_map/dot_general | solution.py:94
  544.6 5.8 %all_to_all.32 = bf16[2,320,2048]{2,1,0:T(8,128)(2,1)S(1)} all-to-all(bf16[2,320,2048]{2,1,0:T(8,128)(2,1)S(1)} %bitcast.80), channel_id=1, replica_groups=mesh['rep'=2,'fs_0'=2,'fs_1'=4,'fs_2'=4,'tp'=2] {'tp'}, dimensions={0} | all-to-all | bytes 5242880 | tf_op jit(solution)/shard_map/all_to_all | solution.py:51
  550.4 0.6 convert_reduce_fusion
  551.0 1.8 add_convert_fusion
  (48 shorter events, 2.4 us)
Async XLA Ops:
  13.4 9.6 %copy-start.3 = (bf16[1024,64]{0,1:T(8,128)(2,1)S(1)}, bf16[1024,64]{0,1:T(8,128)(2,1)}, u32[]{:S(2)}) copy-start(bf16[1024,64]{0,1:T(8,128)(2,1)} %param.17) | copy-start | bytes 393220
  13.4 74.7 %copy-start.2 = (bf16[1408,64]{0,1:T(8,128)(2,1)S(1)}, bf16[1408,64]{0,1:T(8,128)(2,1)}, u32[]{:S(2)}) copy-start(bf16[1408,64]{0,1:T(8,128)(2,1)} %param.21) | copy-start | bytes 540676
  13.4 179.9 %all-to-all-start.3 = ((bf16[32,2,64,1408]{3,2,1,0:T(8,128)(2,1)}), bf16[32,2,64,1408]{3,2,1,0:T(8,128)(2,1)}, u32[]{:S(2)}, u32[]{:S(2)}) async-start(bf16[32,2,64,1408]{3,2,1,0:T(8,128)(2,1)} %stack.26), calls=%async_computation.3 | async-start | bytes 23068672 | tf_op jit(solution)/shard_map/all_to_all | solution.py:80
  22.9 170.4 %copy-start.4 = (bf16[64,1024]{1,0:T(8,128)(2,1)S(1)}, bf16[64,1024]{1,0:T(8,128)(2,1)}, u32[]{:S(2)}) copy-start(bf16[64,1024]{1,0:T(8,128)(2,1)} %param.15) | copy-start | bytes 393220
  22.9 170.4 %copy-start.5 = (bf16[64,1024]{1,0:T(8,128)(2,1)S(1)}, bf16[64,1024]{1,0:T(8,128)(2,1)}, u32[]{:S(2)}) copy-start(bf16[64,1024]{1,0:T(8,128)(2,1)} %param.14) | copy-start | bytes 393220
  22.9 170.3 %copy-start.6 = (bf16[64,1024]{1,0:T(8,128)(2,1)S(1)}, bf16[64,1024]{1,0:T(8,128)(2,1)}, u32[]{:S(2)}) copy-start(bf16[64,1024]{1,0:T(8,128)(2,1)} %param.13) | copy-start | bytes 393220
  22.9 170.3 %all-gather.11.cloned.1.call-start = ((), (), s32[]{:S(2)}) async-start(), calls=%async_computation.6 | async-start | bytes 1310720 | tf_op jit(solution)/shard_map/all_gather | solution.py:32
  88.1 142.6 %all-gather.15.cloned.1.call-start = ((), (), s32[]{:S(2)}) async-start(), calls=%async_computation.8 | async-start | bytes 1802240 | tf_op jit(solution)/shard_map/all_gather | solution.py:32
  94.5 256.9 %all-gather.13.cloned.1.call-start = ((), (), s32[]{:S(2)}) async-start(), calls=%async_computation.7 | async-start | bytes 5242880 | tf_op jit(solution)/shard_map/all_gather | solution.py:32
  199.5 32.6 %copy-start = (bf16[320,2048]{1,0:T(8,128)(2,1)S(1)}, bf16[320,2048]{1,0:T(8,128)(2,1)}, u32[]{:S(2)}) copy-start(bf16[320,2048]{1,0:T(8,128)(2,1)} %param.11) | copy-start | bytes 3932164
  199.5 275.7 %all-to-all-start = ((bf16[32,3,64,1024]{3,2,1,0:T(8,128)(2,1)}), bf16[32,3,64,1024]{3,2,1,0:T(8,128)(2,1)}, u32[]{:S(2)}, u32[]{:S(2)}) async-start(bf16[32,3,64,1024]{3,2,1,0:T(8,128)(2,1)} %stack.22), calls=%async_computation | async-start | bytes 25165824 | tf_op jit(solution)/shard_map/all_to_all | solution.py:80
  230.6 1.9 copy-start.7
  230.6 228.9 %all-gather.17.cloned.1.call-start = ((), (), s32[]{:S(2)}) async-start(), calls=%async_computation.9 | async-start | bytes 7208960 | tf_op jit(solution)/shard_map/all_gather | solution.py:32
  477.1 16.4 %all-to-all-start.1 = ((bf16[2,320,2048]{2,1,0:T(8,128)(2,1)}), bf16[2,320,2048]{2,1,0:T(8,128)(2,1)}, u32[]{:S(2)}, u32[]{:S(2)}) async-start(bf16[2,320,2048]{2,1,0:T(8,128)(2,1)} %broadcast_in_dim.4), calls=%async_computation.1 | async-start | bytes 5242880 | tf_op jit(solution)/shard_map/all_to_all | solution.py:13
  505.5 2.2 copy-start.1
  516.9 1.1 copy-start.8
  516.9 8.3 %slice-start = ((s8[11534336]{0:T(1024)(128)(4,1)}), s8[4194304]{0:T(1024)(128)(4,1)S(1)}, s32[]{:S(2)}) async-start(s8[11534336]{0:T(1024)(128)(4,1)} %bitcast.69), calls=%async_computation.10 | async-start | bytes 8388608
  517.5 7.7 %slice-start.1 = ((s8[11534336]{0:T(1024)(128)(4,1)}), s8[4194304]{0:T(1024)(128)(4,1)S(1)}, s32[]{:S(2)}) async-start(s8[11534336]{0:T(1024)(128)(4,1)} %bitcast.69), calls=%async_computation.11 | async-start | bytes 8388608
  518.5 6.7 %slice-start.2 = ((s8[11534336]{0:T(1024)(128)(4,1)}), s8[3145728]{0:T(1024)(128)(4,1)S(1)}, s32[]{:S(2)}) async-start(s8[11534336]{0:T(1024)(128)(4,1)} %bitcast.69), calls=%async_computation.12 | async-start | bytes 6291456
  518.8 17.9 %slice-start.3 = ((s8[5767168]{0:T(1024)(128)(4,1)}), s8[4194304]{0:T(1024)(128)(4,1)S(1)}, s32[]{:S(2)}) async-start(s8[5767168]{0:T(1024)(128)(4,1)} %bitcast.72), calls=%async_computation.13 | async-start | bytes 8388608
  525.2 11.6 %slice-start.4 = ((s8[5767168]{0:T(1024)(128)(4,1)}), s8[1572864]{0:T(1024)(128)(4,1)S(1)}, s32[]{:S(2)}) async-start(s8[5767168]{0:T(1024)(128)(4,1)} %bitcast.72), calls=%async_computation.14 | async-start | bytes 3145728
Sparse Core Ops, SparseCore 0:
  88.2 104.9 all-gather.10
  194.9 25.2 all-gather.14
  221.8 129.5 all-gather.12
  353.0 106.4 all-gather.16
